TPU v7x, 32 devices: a whole 2x2x4 slice. The times are simulated.
32 devices in a mesh: sp: 8 (over z, y), tp: 4 (over x, core).
Axes of the slice: x: 2, y: 2, z: 4, core: 2. Of those that a mesh axis runs over, the one named last changes fastest.
Arguments:
- tokens: bfloat16 [2048, 4096], P('sp', 'tp'), may hold values from -6 to 6
- input_norm_gain: float32 [4096], replicated, may hold values from 0.1 to 1.9
- query_weight: bfloat16 [4096, 2048], P('sp', 'tp'), may hold values from -0.09375 to 0.09375
- key_weight: bfloat16 [4096, 2048], P('sp', 'tp'), may hold values from -0.09375 to 0.09375
- value_weight: bfloat16 [4096, 2048], P('sp', 'tp'), may hold values from -0.09375 to 0.09375
- decay_first_map: bfloat16 [4096, 128], replicated, may hold values from -0.09375 to 0.09375
- decay_second_map: bfloat16 [128, 2048], P(None, 'tp'), may hold values from -0.5 to 0.5
- channel_decay_offset: float32 [2048], P('tp'), may hold values from -13 to -2
- position_decay_offset: float32 [2048], P('sp'), may hold values from -2 to 2
- extra_log_decay: float32 [2048, 32], P('sp', 'tp'), may hold values from -0.7 to 0
- rate_first_map: bfloat16 [4096, 128], replicated, may hold values from -0.09375 to 0.09375
- rate_second_map: bfloat16 [128, 2048], P(None, 'tp'), may hold values from -0.25 to 0.25
- channel_rate_offset: float32 [2048], P('tp'), may hold values from -10 to 1
- own_term_weight: float32 [2048], P('tp'), may hold values from -2 to 2
- head_norm_gain: float32 [2048], P('tp'), may hold values from 0.1 to 1.9
- starting_state: float32 [32, 64, 64], P('tp'), may hold values from -192 to 192
- outer_gate_weight: bfloat16 [4096, 2048], P('sp', 'tp'), may hold values from -0.09375 to 0.09375
- inner_gate_weight: bfloat16 [4096, 2048], P('sp', 'tp'), may hold values from -0.09375 to 0.09375
- signal_weight: bfloat16 [4096, 2048], P('sp', 'tp'), may hold values from -0.09375 to 0.09375
- convolution_taps: bfloat16 [3, 2048], P(None, 'tp'), may hold values from -3.5 to 3.5
- convolution_gain: float32 [2048], P('tp'), may hold values from 0.1 to 1.9
Outputs:
- linear_attention_output: bfloat16 [2048, 2048], P('sp', 'tp')
- out_conv: bfloat16 [2048, 2048], P('sp', 'tp')
All inputs are finite; a program needn't handle non-finite values.
Results may differ from a plain program's by a relative error of at most 0.009.
Values may be sent and summed in bfloat16 or wider, within the bound.
A program may use at most 128 MiB of HBM per device.

v0:
```python
import jax
import jax.numpy as jnp
from jax import lax
from jax.sharding import PartitionSpec as P

BLOCK = 64


DECAY_FACTOR = 0.606531
NORM_EPS = 1e-06
GROUP_EPS = 0.00064
KEY_EPS = 1e-06


def from_behind(block, axis, distance):
    devices = range(lax.axis_size(axis))
    route = [(i - distance, i) for i in devices if i - distance in devices]
    return lax.ppermute(block, axis, route)


def rounded(values):
    return lax.optimization_barrier(values.astype(jnp.bfloat16)).astype(jnp.float32)


def contract(spec, left, right):
    return jnp.einsum(spec, left, right, precision=lax.Precision.HIGHEST)


def fold_rows(normed):

    def accumulate(totals, pieces, offset):
        return tuple(
            (
                jnp.dot(normed, weight_piece, preferred_element_type=jnp.float32)
                for weight_piece in pieces
            )
        )

    return accumulate


def mixer_blocks(query, keyed, valued, unit_key, decay_logarithm, rate):
    sequence_length, number_heads, head_dimension = query.shape
    block_size = BLOCK
    count = sequence_length // block_size
    eye_heads = jnp.broadcast_to(
        jnp.eye(head_dimension, dtype=jnp.float32), (number_heads, head_dimension, head_dimension)
    )
    eye_block = jnp.eye(block_size, dtype=jnp.float32)
    later = jnp.arange(block_size)[:, None]
    earlier = jnp.arange(block_size)[None, :]
    strict = later > earlier
    inclusive = later >= earlier
    block_shape = (count, block_size, number_heads, head_dimension)
    query_b, keyed_b, valued_b, unit_b, decay_b, rate_b = (
        values.reshape(block_shape)
        for values in (query, keyed, valued, unit_key, decay_logarithm, rate)
    )
    cumul = jnp.cumsum(decay_b, axis=1)
    before = cumul - decay_b
    a_prime = -unit_b * jnp.exp(before)
    b_scaled = unit_b * rate_b * jnp.exp(-cumul)
    k_scaled = keyed_b * jnp.exp(-cumul)
    r_prime = query_b * jnp.exp(cumul)
    removal = jnp.where(strict, contract("cthn,cshn->chts", a_prime, b_scaled), 0.0)
    writes = jnp.where(strict, contract("cthn,cshn->chts", a_prime, k_scaled), 0.0)
    reads = jnp.where(inclusive, contract("cthn,cshn->chts", r_prime, b_scaled), 0.0)
    key_reads = jnp.where(inclusive, contract("cthn,cshn->chts", r_prime, k_scaled), 0.0)
    power = removal
    inverse = eye_block + removal
    reach = 2
    while reach < block_size:
        power = contract("chts,chsu->chtu", power, power)
        inverse = inverse + contract("chts,chsu->chtu", inverse, power)
        reach = reach * 2
    unit_solved = contract("chts,cshn->chtn", inverse, a_prime)
    free_solved = contract(
        "chts,chsv->chtv", inverse, contract("chts,cshv->chtv", writes, valued_b)
    )
    probe_raw = jnp.transpose(r_prime, (0, 2, 1, 3)) + contract(
        "chts,chsn->chtn", reads, unit_solved
    )
    free_read = contract("chts,chsv->chtv", reads, free_solved) + contract(
        "chts,cshv->chtv", key_reads, valued_b
    )
    closing = jnp.exp(cumul[:, -1])
    b_end = b_scaled * closing[:, None]
    k_end = k_scaled * closing[:, None]
    step_map = eye_heads[None] * closing[:, :, None, :] + contract(
        "chtj,cthk->chjk", unit_solved, b_end
    )
    constant = contract("chtv,cthk->chvk", free_solved, b_end) + contract(
        "cthv,cthk->chvk", valued_b, k_end
    )
    local_state = jnp.zeros((number_heads, head_dimension, head_dimension), jnp.float32)
    product = eye_heads
    entering_states = []
    entering_maps = []
    for index in range(count):
        entering_states.append(local_state)
        entering_maps.append(product)
        local_state = contract("hvk,hkj->hvj", local_state, step_map[index]) + constant[index]
        product = contract("hij,hjk->hik", product, step_map[index])
    stacked_states = jnp.stack(entering_states)
    stacked_maps = jnp.stack(entering_maps)
    recalled = contract("chvk,chtk->cthv", stacked_states, probe_raw) + jnp.transpose(
        free_read, (0, 2, 1, 3)
    )
    probe = contract("chjk,chtk->cthj", stacked_maps, probe_raw)
    head_shape = (sequence_length, number_heads, head_dimension)
    return (recalled.reshape(head_shape), probe.reshape(head_shape), local_state, product)


def mixer_local(
    normed,
    projected,
    decay_first_map,
    decay_second_map,
    channel_decay_offset,
    position_decay_offset,
    extra_log_decay,
    rate_first_map,
    rate_second_map,
    channel_rate_offset,
):
    query, keyed, valued = (rounded(values) for values in projected)
    sequence_length = normed.shape[0]
    number_heads = extra_log_decay.shape[1]
    head_dimension = query.shape[1] // number_heads
    decay_low = jnp.tanh(
        jnp.dot(normed, decay_first_map, preferred_element_type=jnp.float32)
    ).astype(jnp.bfloat16)
    decay_logits = (
        channel_decay_offset
        + jnp.dot(decay_low, decay_second_map, preferred_element_type=jnp.float32)
        + position_decay_offset[:, None]
    )
    decay_logarithm = -DECAY_FACTOR * jax.nn.sigmoid(decay_logits) + jnp.repeat(
        extra_log_decay, head_dimension, axis=1
    )
    rate_low = jnp.dot(normed, rate_first_map, preferred_element_type=jnp.float32).astype(
        jnp.bfloat16
    )
    rate = jax.nn.sigmoid(
        channel_rate_offset + jnp.dot(rate_low, rate_second_map, preferred_element_type=jnp.float32)
    )
    head_shape = (sequence_length, number_heads, head_dimension)
    query_per_head = query.reshape(head_shape)
    key_per_head = keyed.reshape(head_shape)
    value_per_head = valued.reshape(head_shape)
    unit_key = key_per_head * lax.rsqrt(
        jnp.sum(key_per_head * key_per_head, axis=2, keepdims=True) + KEY_EPS
    )
    recalled, probe, final_state, final_product = mixer_blocks(
        query_per_head,
        key_per_head,
        value_per_head,
        unit_key,
        decay_logarithm.reshape(head_shape),
        rate.reshape(head_shape),
    )
    return (
        (query_per_head, key_per_head, value_per_head),
        recalled,
        probe,
        final_state,
        final_product,
    )


def shards(
    tokens,
    input_norm_gain,
    query_weight,
    key_weight,
    value_weight,
    decay_first_map,
    decay_second_map,
    channel_decay_offset,
    position_decay_offset,
    extra_log_decay,
    rate_first_map,
    rate_second_map,
    channel_rate_offset,
    own_term_weight,
    head_norm_gain,
    starting_state,
    outer_gate_weight,
    inner_gate_weight,
    signal_weight,
    convolution_taps,
    convolution_gain,
):
    whole = lax.all_gather(tokens, "tp", axis=1, tiled=True)
    wide = whole.astype(jnp.float32)
    normed = (
        wide * lax.rsqrt(jnp.mean(wide * wide, axis=1, keepdims=True) + NORM_EPS) * input_norm_gain
    ).astype(jnp.bfloat16)
    sequence_length = normed.shape[0]
    accumulate = fold_rows(normed)
    empty = jnp.zeros((sequence_length, query_weight.shape[1]), jnp.float32)
    mixer_args = (
        decay_first_map,
        decay_second_map,
        channel_decay_offset,
        position_decay_offset,
        extra_log_decay,
        rate_first_map,
        rate_second_map,
        channel_rate_offset,
    )
    query, keyed, valued, outer, inner, signal = accumulate(
        (empty, empty, empty, empty, empty, empty),
        (
            lax.all_gather(query_weight, "sp", axis=0, tiled=True),
            lax.all_gather(key_weight, "sp", axis=0, tiled=True),
            lax.all_gather(value_weight, "sp", axis=0, tiled=True),
            lax.all_gather(outer_gate_weight, "sp", axis=0, tiled=True),
            lax.all_gather(inner_gate_weight, "sp", axis=0, tiled=True),
            lax.all_gather(signal_weight, "sp", axis=0, tiled=True),
        ),
        jnp.int32(0),
    )
    mixer = mixer_local(normed, (query, keyed, valued), *mixer_args)
    (query_per_head, key_per_head, value_per_head), recalled, probe, final_state, final_product = (
        mixer
    )
    number_heads, head_dimension = (query_per_head.shape[1], query_per_head.shape[2])
    position = lax.axis_index("sp")

    def hand_on(turn, entering_now):
        outgoing = contract("hvk,hkj->hvj", entering_now, final_product) + final_state
        moved = from_behind(outgoing.astype(jnp.bfloat16), "sp", 1).astype(outgoing.dtype)
        return jnp.where(position == 0, starting_state, moved)

    entering = lax.fori_loop(0, lax.axis_size("sp") - 1, hand_on, starting_state)
    recalled = recalled + contract("hvk,thk->thv", entering, probe)
    center = recalled - jnp.mean(recalled, axis=2, keepdims=True)
    variance = jnp.mean(center * center, axis=2, keepdims=True)
    input_normed = (
        center
        * lax.rsqrt(variance + GROUP_EPS)
        * head_norm_gain.reshape(number_heads, head_dimension)
    )
    own_term = (
        jnp.sum(
            query_per_head * key_per_head * own_term_weight.reshape(number_heads, head_dimension),
            axis=2,
            keepdims=True,
        )
        * value_per_head
    )
    linear_attention_output = (
        (input_normed + own_term)
        .reshape(sequence_length, number_heads * head_dimension)
        .astype(jnp.bfloat16)
    )
    outer_f = rounded(outer)
    mixed_in = (rounded(inner) * rounded(signal)).astype(jnp.bfloat16)
    previous = from_behind(mixed_in[sequence_length - 2 :], "sp", 1)
    padded = jnp.concatenate([previous, mixed_in], axis=0).astype(jnp.float32)
    taps = convolution_taps.astype(jnp.float32)
    gated = outer_f * (taps[0] * padded[:-2] + taps[1] * padded[1:-1] + taps[2] * padded[2:])
    squares = lax.psum(jnp.sum(gated * gated, axis=1), "tp")
    channel_total = gated.shape[1] * lax.axis_size("tp")
    out_conv = (
        gated * lax.rsqrt(squares[:, None] / channel_total + NORM_EPS) * convolution_gain
    ).astype(jnp.bfloat16)
    return (linear_attention_output, out_conv)


def solution(mesh):
    placed = (
        P("sp", "tp"),
        P(),
        P("sp", "tp"),
        P("sp", "tp"),
        P("sp", "tp"),
        P(),
        P(None, "tp"),
        P("tp"),
        P("sp"),
        P("sp", "tp"),
        P(),
        P(None, "tp"),
        P("tp"),
        P("tp"),
        P("tp"),
        P("tp", None, None),
        P("sp", "tp"),
        P("sp", "tp"),
        P("sp", "tp"),
        P(None, "tp"),
        P("tp"),
    )
    return jax.shard_map(
        shards,
        mesh=mesh,
        in_specs=placed,
        out_specs=(P("sp", "tp"), P("sp", "tp")),
        check_vma=False,
    )
```

profile of v0, /device:TPU:0, one launch (start us, length us, event | category | flops | bytes accessed | tf_op | source)
XLA Modules:
  0.0 508.4 jit_solution(5664682041117537056)
XLA Ops:
  13.2 21.7 %all-gather.8.cloned.1.call-done = bf16[256,4096]{1,0:T(8,128)(2,1)} async-done(((bf16[256,1024]{1,0:T(8,128)(2,1)}), bf16[256,4096]{1,0:T(8,128)(2,1)}) %all-gather.8.cloned.1.call-update) | async-done | bytes 2097168 | tf_op jit(solution)/shard_map/all_gather | solution.py:194
  35.0 2.1 fusion.2
  37.1 2.6 fusion.17
  40.0 26.4 %fusion.87 = f32[4,64,8,64]{3,2,1,0:T(8,128)S(1)} fusion(f32[4,64,8,64]{3,2,1,0:T(8,128)S(1)} %reshape_reshape.14), kind=kOutput, calls=%fused_computation.144 | output fusion | flops 8257536 | bytes 1048576 | tf_op jit(solution)/shard_map/jit(cumsum)/reduce_window_sum | solution.py:59
  66.4 2.9 fusion.19
  70.5 39.4 %all-gather.12.cloned.1.call-done = bf16[4096,512]{1,0:T(8,128)(2,1)} async-done(((bf16[512,512]{1,0:T(8,128)(2,1)}), bf16[4096,512]{1,0:T(8,128)(2,1)}) %all-gather.12.cloned.1.call-update) | async-done | bytes 4194320 | tf_op jit(solution)/shard_map/all_gather | solution.py:216
  109.9 4.1 convolution_convert_fusion.4
  114.0 69.4 %all-gather.10.cloned.1.call-done = bf16[4096,512]{1,0:T(8,128)(2,1)} async-done(((bf16[512,512]{1,0:T(8,128)(2,1)}), bf16[4096,512]{1,0:T(8,128)(2,1)}) %all-gather.10.cloned.1.call-update) | async-done | bytes 4194320 | tf_op jit(solution)/shard_map/all_gather | solution.py:215
  183.5 4.1 convolution_convert_fusion.5
  191.1 65.6 %all-gather.14.cloned.1.call-done = bf16[4096,512]{1,0:T(8,128)(2,1)} async-done(((bf16[512,512]{1,0:T(8,128)(2,1)}), bf16[4096,512]{1,0:T(8,128)(2,1)}) %all-gather.14.cloned.1.call-update) | async-done | bytes 4194320 | tf_op jit(solution)/shard_map/all_gather | solution.py:217
  256.8 4.8 convolution_convert_fusion.3
  261.6 1.9 copy.82
  263.5 2.1 reshape_reshape.16
  265.6 2.1 copy.62
  269.6 3.1 broadcast_multiply_fusion.1
  272.7 2.1 convolution_select_fusion.2
  288.4 2.0 convolution_select_fusion.1
  292.5 2.2 convolution_select_fusion.3
  296.3 2.9 convolution_add_fusion.8
  299.2 2.9 fusion.41
  302.1 2.2 fusion.94
  304.2 3.6 convolution_select_fusion
  307.9 2.1 copy.81
  310.0 2.7 convolution_add_fusion.7
  314.1 1.9 fusion.23
  322.6 1.8 convolution_bitcast_fusion
  326.3 3.9 all-gather.20.cloned.1.call-done
  330.1 4.1 convolution_convert_fusion
  334.3 69.2 %all-gather.18.cloned.1.call-done = bf16[4096,512]{1,0:T(8,128)(2,1)} async-done(((bf16[512,512]{1,0:T(8,128)(2,1)}), bf16[4096,512]{1,0:T(8,128)(2,1)}) %all-gather.18.cloned.1.call-update) | async-done | bytes 4194320 | tf_op jit(solution)/shard_map/all_gather | solution.py:219
  403.5 4.1 convolution_convert_fusion.1
  407.7 2.6 collective-permute-start.1
  412.1 74.2 %while.12 = (s32[]{:T(128)}, f32[8,64,64]{2,1,0:T(8,128)S(1)}, pred[]{:T(512)}, f32[8,64,64]{2,1,0:T(8,128)S(1)}, f32[8,64,64]{2,1,0:T(8,128)S(1)}, /*index=5*/f32[8,64,64]{2,1,0:T(8,128)S(1)}, s32[]{:T(128)}) while((s32[]{:T(128)}, f32[8,64,64]{2,1,0:T(8,128)S(1)}, pred[]{:T(512)}, f32[8,64,64]{2,1,0:T(8,128)S(1)}, ...), condition=%wide.region_4.5_spmd, body=%wide.region_3.4_spmd.sunk | while | flops 25296896 | bytes 1048694 | solution.py:236
  412.5 4.0 collective-permute-start
  416.5 4.7 collective-permute-done
  421.7 4.4 collective-permute-start
  426.1 2.5 collective-permute-done
  429.0 7.0 %collective-permute-start = (bf16[8,64,64]{2,1,0:T(8,128)(2,1)S(1)}, bf16[8,64,64]{2,1,0:T(8,128)(2,1)S(1)}, u32[]{:S(2)}, u32[]{:S(2)}) collective-permute-start(bf16[8,64,64]{2,1,0:T(8,128)(2,1)S(1)} %fusion.153), channel_id=1, source_target_pairs={{0,4},{4,8},{8,12},{12,16},{16,20},{20,24},{24,28},{1,5},{5,9},{9,... | collective-permute-start | bytes 196616 | tf_op jit(solution)/shard_map/while/body/eval_jaxpr/ppermute | solution.py:18
  436.1 2.5 collective-permute-done
  439.0 5.3 %collective-permute-start = (bf16[8,64,64]{2,1,0:T(8,128)(2,1)S(1)}, bf16[8,64,64]{2,1,0:T(8,128)(2,1)S(1)}, u32[]{:S(2)}, u32[]{:S(2)}) collective-permute-start(bf16[8,64,64]{2,1,0:T(8,128)(2,1)S(1)} %fusion.153), channel_id=1, source_target_pairs={{0,4},{4,8},{8,12},{12,16},{16,20},{20,24},{24,28},{1,5},{5,9},{9,... | collective-permute-start | bytes 196616 | tf_op jit(solution)/shard_map/while/body/eval_jaxpr/ppermute | solution.py:18
  444.3 5.4 %collective-permute-done = bf16[8,64,64]{2,1,0:T(8,128)(2,1)S(1)} collective-permute-done((bf16[8,64,64]{2,1,0:T(8,128)(2,1)S(1)}, bf16[8,64,64]{2,1,0:T(8,128)(2,1)S(1)}, u32[]{:S(2)}, u32[]{:S(2)}) %collective-permute-start) | collective-permute-done | bytes 65568 | tf_op jit(solution)/shard_map/while/body/eval_jaxpr/ppermute | solution.py:18
  450.1 5.3 %collective-permute-start = (bf16[8,64,64]{2,1,0:T(8,128)(2,1)S(1)}, bf16[8,64,64]{2,1,0:T(8,128)(2,1)S(1)}, u32[]{:S(2)}, u32[]{:S(2)}) collective-permute-start(bf16[8,64,64]{2,1,0:T(8,128)(2,1)S(1)} %fusion.153), channel_id=1, source_target_pairs={{0,4},{4,8},{8,12},{12,16},{16,20},{20,24},{24,28},{1,5},{5,9},{9,... | collective-permute-start | bytes 196616 | tf_op jit(solution)/shard_map/while/body/eval_jaxpr/ppermute | solution.py:18
  455.4 5.4 %collective-permute-done = bf16[8,64,64]{2,1,0:T(8,128)(2,1)S(1)} collective-permute-done((bf16[8,64,64]{2,1,0:T(8,128)(2,1)S(1)}, bf16[8,64,64]{2,1,0:T(8,128)(2,1)S(1)}, u32[]{:S(2)}, u32[]{:S(2)}) %collective-permute-start) | collective-permute-done | bytes 65568 | tf_op jit(solution)/shard_map/while/body/eval_jaxpr/ppermute | solution.py:18
  461.2 8.1 %collective-permute-start = (bf16[8,64,64]{2,1,0:T(8,128)(2,1)S(1)}, bf16[8,64,64]{2,1,0:T(8,128)(2,1)S(1)}, u32[]{:S(2)}, u32[]{:S(2)}) collective-permute-start(bf16[8,64,64]{2,1,0:T(8,128)(2,1)S(1)} %fusion.153), channel_id=1, source_target_pairs={{0,4},{4,8},{8,12},{12,16},{16,20},{20,24},{24,28},{1,5},{5,9},{9,... | collective-permute-start | bytes 196616 | tf_op jit(solution)/shard_map/while/body/eval_jaxpr/ppermute | solution.py:18
  469.3 3.2 collective-permute-done
  472.9 10.9 %collective-permute-start = (bf16[8,64,64]{2,1,0:T(8,128)(2,1)S(1)}, bf16[8,64,64]{2,1,0:T(8,128)(2,1)S(1)}, u32[]{:S(2)}, u32[]{:S(2)}) collective-permute-start(bf16[8,64,64]{2,1,0:T(8,128)(2,1)S(1)} %fusion.153), channel_id=1, source_target_pairs={{0,4},{4,8},{8,12},{12,16},{16,20},{20,24},{24,28},{1,5},{5,9},{9,... | collective-permute-start | bytes 196616 | tf_op jit(solution)/shard_map/while/body/eval_jaxpr/ppermute | solution.py:18
  483.8 2.5 collective-permute-done
  488.3 4.2 convolution_convert_fusion.2
  494.0 6.6 %psum.7 = f32[256]{0:T(256)S(1)} all-reduce(f32[256]{0:T(256)S(1)} %get-tuple-element.93), channel_id=1, replica_groups=mesh['sp'=8,'tp'=4] {'tp'}, use_global_device_ids=true, to_apply=%region_9.10 | all-reduce | flops 256 | bytes 2048 | tf_op jit(solution)/shard_map/psum | solution.py:264
  (148 shorter events, 48.4 us)
Async XLA Ops:
  7.2 29.9 %copy-start = (bf16[4096,128]{1,0:T(8,128)(2,1)S(1)}, bf16[4096,128]{1,0:T(8,128)(2,1)}, u32[]{:S(2)}) copy-start(bf16[4096,128]{1,0:T(8,128)(2,1)} %param.28) | copy-start | bytes 3145732
  7.2 5.8 %copy-start.3 = (f32[8,64,64]{2,1,0:T(8,128)S(1)}, f32[8,64,64]{2,1,0:T(8,128)}, u32[]{:S(2)}) copy-start(f32[8,64,64]{2,1,0:T(8,128)} %param.38) | copy-start | bytes 393220
  7.2 5.8 %copy-start.21 = (f32[512]{0:T(512)S(1)}, f32[512]{0:T(512)}, u32[]{:S(2)}) copy-start(f32[512]{0:T(512)} %param.36) | copy-start | bytes 6148
  7.2 5.9 %copy-start.22 = (f32[512]{0:T(512)S(1)}, f32[512]{0:T(512)}, u32[]{:S(2)}) copy-start(f32[512]{0:T(512)} %param.37) | copy-start | bytes 6148
  7.2 6.0 %copy-start.19 = (bf16[3,512]{1,0:T(4,128)(2,1)S(1)}, bf16[3,512]{1,0:T(4,128)(2,1)}, u32[]{:S(2)}) copy-start(bf16[3,512]{1,0:T(4,128)(2,1)} %param.42) | copy-start | bytes 9220
  7.2 29.8 %copy-start.25 = (f32[4096]{0:T(1024)S(1)}, f32[4096]{0:T(1024)}, u32[]{:S(2)}) copy-start(f32[4096]{0:T(1024)} %param.24) | copy-start | bytes 49156
  7.2 29.8 %copy-start.23 = (bf16[128,512]{1,0:T(8,128)(2,1)S(1)}, bf16[128,512]{1,0:T(8,128)(2,1)}, u32[]{:S(2)}) copy-start(bf16[128,512]{1,0:T(8,128)(2,1)} %param.29) | copy-start | bytes 393220
  7.2 29.8 %copy-start.28 = (f32[256]{0:T(256)S(1)}, f32[256]{0:T(256)}, u32[]{:S(2)}) copy-start(f32[256]{0:T(256)} %param.31) | copy-start | bytes 3076
  7.3 29.8 %copy-start.26 = (f32[512]{0:T(512)S(1)}, f32[512]{0:T(512)}, u32[]{:S(2)}) copy-start(f32[512]{0:T(512)} %param.30) | copy-start | bytes 6148
  7.3 27.7 %all-gather.8.cloned.1.call-start = ((), (), s32[]{:S(2)}) async-start(), calls=%async_computation | async-start | bytes 2621440 | tf_op jit(solution)/shard_map/all_gather | solution.py:194
  8.0 101.9 %all-gather.12.cloned.1.call-start = ((), (), s32[]{:S(2)}) async-start(), calls=%async_computation.2 | async-start | bytes 4718592 | tf_op jit(solution)/shard_map/all_gather | solution.py:216
  8.7 174.7 %all-gather.10.cloned.1.call-start = ((), (), s32[]{:S(2)}) async-start(), calls=%async_computation.1 | async-start | bytes 4718592 | tf_op jit(solution)/shard_map/all_gather | solution.py:215
  9.5 247.3 %all-gather.14.cloned.1.call-start = ((), (), s32[]{:S(2)}) async-start(), calls=%async_computation.3 | async-start | bytes 4718592 | tf_op jit(solution)/shard_map/all_gather | solution.py:217
  10.1 320.1 %all-gather.20.cloned.1.call-start = ((), (), s32[]{:S(2)}) async-start(), calls=%async_computation.6 | async-start | bytes 4718592 | tf_op jit(solution)/shard_map/all_gather | solution.py:220
  10.6 392.8 %all-gather.18.cloned.1.call-start = ((), (), s32[]{:S(2)}) async-start(), calls=%async_computation.5 | async-start | bytes 4718592 | tf_op jit(solution)/shard_map/all_gather | solution.py:219
  11.2 477.1 %all-gather.16.cloned.1.call-start = ((), (), s32[]{:S(2)}) async-start(), calls=%async_computation.4 | async-start | bytes 4718592 | tf_op jit(solution)/shard_map/all_gather | solution.py:218
  37.1 29.3 %copy-start.24 = (bf16[128,512]{1,0:T(8,128)(2,1)S(1)}, bf16[128,512]{1,0:T(8,128)(2,1)}, u32[]{:S(2)}) copy-start(bf16[128,512]{1,0:T(8,128)(2,1)} %param.34) | copy-start | bytes 393220
  37.1 29.3 %copy-start.27 = (f32[512]{0:T(512)S(1)}, f32[512]{0:T(512)}, u32[]{:S(2)}) copy-start(f32[512]{0:T(512)} %param.35) | copy-start | bytes 6148
  187.6 1.2 copy-start.18
  285.9 4.5 copy-start.5
  307.9 4.8 copy-start.2
  310.0 6.0 %copy-start.6 = (bf16[4,64,8,64]{3,2,1,0:T(8,128)(2,1)S(1)}, bf16[4,64,8,64]{3,2,1,0:T(8,128)(2,1)}, u32[]{:S(2)}) copy-start(bf16[4,64,8,64]{3,2,1,0:T(8,128)(2,1)} %reshape_reshape.16) | copy-start | bytes 786436
  310.0 6.0 %copy-start.8 = (f32[4,8,64,64]{3,2,1,0:T(8,128)S(1)}, f32[4,8,64,64]{3,2,1,0:T(8,128)}, u32[]{:S(2)}) copy-start(f32[4,8,64,64]{3,2,1,0:T(8,128)} %fusion.94) | copy-start | bytes 1572868
  310.0 6.0 %copy-start.9 = (f32[4,8,64,64]{3,2,1,0:T(8,128)S(1)}, f32[4,8,64,64]{3,2,1,0:T(8,128)}, u32[]{:S(2)}) copy-start(f32[4,8,64,64]{3,2,1,0:T(8,128)} %convolution_select_fusion) | copy-start | bytes 1572868
  312.7 1.0 copy-start.7
  314.1 1.9 copy-start.12
  321.9 0.7 copy-start.10
  334.3 76.1 %copy-start.11 = (f32[8,64,64]{2,1,0:T(8,128)S(1)}, f32[8,64,64]{2,1,0:T(8,128)}, u32[]{:S(2)}) copy-start(f32[8,64,64]{2,1,0:T(8,128)} %copy-done.10) | copy-start | bytes 393220
  334.3 76.4 %copy-start.13 = (f32[8,64,64]{2,1,0:T(8,128)S(1)}, f32[8,64,64]{2,1,0:T(8,128)}, u32[]{:S(2)}) copy-start(f32[8,64,64]{2,1,0:T(8,128)} %copy-done.12) | copy-start | bytes 393220
  334.3 77.8 %copy-start.4 = (f32[8,64,64]{2,1,0:T(8,128)S(1)}, f32[8,64,64]{2,1,0:T(8,128)}, u32[]{:S(2)}) copy-start(f32[8,64,64]{2,1,0:T(8,128)} %param.38) | copy-start | bytes 393220
  407.7 86.0 %collective-permute-start.1 = (bf16[2,512]{1,0:T(2,128)(2,1)S(1)}, bf16[2,512]{1,0:T(2,128)(2,1)S(1)}, u32[]{:S(2)}, u32[]{:S(2)}) collective-permute-start(bf16[2,512]{1,0:T(2,128)(2,1)S(1)} %slice.78), channel_id=1, source_target_pairs={{0,4},{4,8},{8,12},{12,16},{16,20},{20,24},{24,28},{1,5},{5,9},{9,... | collective-permute-start | bytes 6152 | tf_op jit(solution)/shard_map/ppermute | solution.py:18
  412.1 74.2 %copy-start.14 = (f32[256,8,64]{0,2,1:T(8,128)S(1)}, f32[256,8,64]{0,2,1:T(8,128)}, u32[]{:S(2)}) copy-start(f32[256,8,64]{0,2,1:T(8,128)} %reshape.89) | copy-start | bytes 1572868
  412.1 74.2 %copy-start.15 = (f32[256,8,64]{0,2,1:T(8,128)S(1)}, f32[256,8,64]{0,2,1:T(8,128)}, u32[]{:S(2)}) copy-start(f32[256,8,64]{0,2,1:T(8,128)} %reshape.90) | copy-start | bytes 1572868
  412.5 8.7 %collective-permute-start = (bf16[8,64,64]{2,1,0:T(8,128)(2,1)S(1)}, bf16[8,64,64]{2,1,0:T(8,128)(2,1)S(1)}, u32[]{:S(2)}, u32[]{:S(2)}) collective-permute-start(bf16[8,64,64]{2,1,0:T(8,128)(2,1)S(1)} %fusion.153), channel_id=1, source_target_pairs={{0,4},{4,8},{8,12},{12,16},{16,20},{20,24},{24,28},{1,5},{5,9},{9,... | collective-permute-start | bytes 196616 | tf_op jit(solution)/shard_map/while/body/eval_jaxpr/ppermute | solution.py:18
  421.7 6.9 %collective-permute-start = (bf16[8,64,64]{2,1,0:T(8,128)(2,1)S(1)}, bf16[8,64,64]{2,1,0:T(8,128)(2,1)S(1)}, u32[]{:S(2)}, u32[]{:S(2)}) collective-permute-start(bf16[8,64,64]{2,1,0:T(8,128)(2,1)S(1)} %fusion.153), channel_id=1, source_target_pairs={{0,4},{4,8},{8,12},{12,16},{16,20},{20,24},{24,28},{1,5},{5,9},{9,... | collective-permute-start | bytes 196616 | tf_op jit(solution)/shard_map/while/body/eval_jaxpr/ppermute | solution.py:18
  429.0 9.5 %collective-permute-start = (bf16[8,64,64]{2,1,0:T(8,128)(2,1)S(1)}, bf16[8,64,64]{2,1,0:T(8,128)(2,1)S(1)}, u32[]{:S(2)}, u32[]{:S(2)}) collective-permute-start(bf16[8,64,64]{2,1,0:T(8,128)(2,1)S(1)} %fusion.153), channel_id=1, source_target_pairs={{0,4},{4,8},{8,12},{12,16},{16,20},{20,24},{24,28},{1,5},{5,9},{9,... | collective-permute-start | bytes 196616 | tf_op jit(solution)/shard_map/while/body/eval_jaxpr/ppermute | solution.py:18
  439.0 10.7 %collective-permute-start = (bf16[8,64,64]{2,1,0:T(8,128)(2,1)S(1)}, bf16[8,64,64]{2,1,0:T(8,128)(2,1)S(1)}, u32[]{:S(2)}, u32[]{:S(2)}) collective-permute-start(bf16[8,64,64]{2,1,0:T(8,128)(2,1)S(1)} %fusion.153), channel_id=1, source_target_pairs={{0,4},{4,8},{8,12},{12,16},{16,20},{20,24},{24,28},{1,5},{5,9},{9,... | collective-permute-start | bytes 196616 | tf_op jit(solution)/shard_map/while/body/eval_jaxpr/ppermute | solution.py:18
  450.1 10.7 %collective-permute-start = (bf16[8,64,64]{2,1,0:T(8,128)(2,1)S(1)}, bf16[8,64,64]{2,1,0:T(8,128)(2,1)S(1)}, u32[]{:S(2)}, u32[]{:S(2)}) collective-permute-start(bf16[8,64,64]{2,1,0:T(8,128)(2,1)S(1)} %fusion.153), channel_id=1, source_target_pairs={{0,4},{4,8},{8,12},{12,16},{16,20},{20,24},{24,28},{1,5},{5,9},{9,... | collective-permute-start | bytes 196616 | tf_op jit(solution)/shard_map/while/body/eval_jaxpr/ppermute | solution.py:18
  461.2 11.2 %collective-permute-start = (bf16[8,64,64]{2,1,0:T(8,128)(2,1)S(1)}, bf16[8,64,64]{2,1,0:T(8,128)(2,1)S(1)}, u32[]{:S(2)}, u32[]{:S(2)}) collective-permute-start(bf16[8,64,64]{2,1,0:T(8,128)(2,1)S(1)} %fusion.153), channel_id=1, source_target_pairs={{0,4},{4,8},{8,12},{12,16},{16,20},{20,24},{24,28},{1,5},{5,9},{9,... | collective-permute-start | bytes 196616 | tf_op jit(solution)/shard_map/while/body/eval_jaxpr/ppermute | solution.py:18
  472.9 13.4 %collective-permute-start = (bf16[8,64,64]{2,1,0:T(8,128)(2,1)S(1)}, bf16[8,64,64]{2,1,0:T(8,128)(2,1)S(1)}, u32[]{:S(2)}, u32[]{:S(2)}) collective-permute-start(bf16[8,64,64]{2,1,0:T(8,128)(2,1)S(1)} %fusion.153), channel_id=1, source_target_pairs={{0,4},{4,8},{8,12},{12,16},{16,20},{20,24},{24,28},{1,5},{5,9},{9,... | collective-permute-start | bytes 196616 | tf_op jit(solution)/shard_map/while/body/eval_jaxpr/ppermute | solution.py:18
  487.1 5.5 %copy-start.16 = (f32[256,512]{0,1:T(8,128)S(1)}, f32[256,512]{0,1:T(8,128)}, u32[]{:S(2)}) copy-start(f32[256,512]{0,1:T(8,128)} %copy.82) | copy-start | bytes 1572868
  487.1 5.5 %copy-start.17 = (f32[256,512]{0,1:T(8,128)S(1)}, f32[256,512]{0,1:T(8,128)}, u32[]{:S(2)}) copy-start(f32[256,512]{0,1:T(8,128)} %copy.81) | copy-start | bytes 1572868
  488.3 13.1 %copy-start.1 = (bf16[4096,128]{1,0:T(8,128)(2,1)S(1)}, bf16[4096,128]{1,0:T(8,128)(2,1)}, u32[]{:S(2)}) copy-start(bf16[4096,128]{1,0:T(8,128)(2,1)} %param.28) | copy-start | bytes 3145732
  492.5 8.1 %copy-start.20 = (f32[512]{0:T(512)S(1)}, f32[512]{0:T(512)}, u32[]{:S(2)}) copy-start(f32[512]{0:T(512)} %param.43) | copy-start | bytes 6148
Sparse Core Ops, SparseCore 0:
  9.6 25.2 all-gather.7
  37.1 72.7 all-gather.11
  112.1 71.3 all-gather.9
  185.4 71.3 all-gather.13
  258.8 71.3 all-gather.19
  332.1 71.3 all-gather.17
  405.6 82.6 all-gather.15
where the time goes:
time: 519 us; the launch traced here: 508 us
  waiting for transfers between devices  301 us (58%)
  matrix products  81.4 us (16%)
  starting transfers between devices  47.9 us (9%)
  other arithmetic  35.6 us (7%)
  local copies, waits for them, and re-layouts  20.6 us (4%)
  between operations  15.1 us (3%)
  blocking collectives  6.56 us (1%)
    all_gather x1, waiting for transfers between devices, shards(): lax.all_gather(query_weight, 'sp', axis=0, tiled=True)  69.4 us
    all_gather x1, waiting for transfers between devices, shards(): lax.all_gather(inner_gate_weight, 'sp', axis=0, tiled=True)  69.2 us
    all_gather x1, waiting for transfers between devices, shards(): lax.all_gather(value_weight, 'sp', axis=0, tiled=True)  65.6 us
    dot_general x41, matrix products, contract(): return jnp.einsum(spec, left, right, precision=lax.Precision.HIGHEST)  50.4 us
    ppermute x8, starting transfers between devices, from_behind(): return lax.ppermute(block, axis, route)  47.6 us
    all_gather x1, waiting for transfers between devices, shards(): lax.all_gather(key_weight, 'sp', axis=0, tiled=True)  39.4 us
    another operation x1, other arithmetic, mixer_blocks(): cumul = jnp.cumsum(decay_b, axis=1)  26.4 us
    ppermute x8, waiting for transfers between devices, from_behind(): return lax.ppermute(block, axis, route)  26.1 us
  transfers between devices with their start and end apart: 15, of which 14 were waited for; matrix products, arithmetic and copies ran while one was open for 27% of the time, Pallas kernels for 0%

commit v1 on v0

--- a/solution.py
+++ b/solution.py
@@ -1,6 +1,10 @@
+import functools
+
 import jax
 import jax.numpy as jnp
 from jax import lax
+from jax.experimental import pallas as pl
+from jax.experimental.pallas import tpu as pltpu
 from jax.sharding import PartitionSpec as P
 
 BLOCK = 64
@@ -269,6 +273,286 @@
     return (linear_attention_output, out_conv)
 
 
+HEAD_ROWS = 8
+
+
+def head_kernel(
+    x_ref, w_ref, pos_ref, extra_ref, decay_map_ref, rate_map_ref, chan_ref, start_ref,
+    lin_ref, gated_ref, state_ref, conv_ref,
+):
+    f32, bf16 = jnp.float32, jnp.bfloat16
+    spans, pieces, rows, depth = x_ref.shape
+    positions = spans * rows
+    size = start_ref.shape[0]
+    count = positions // BLOCK
+
+    @pl.when(pl.program_id(0) == 0)
+    def _():
+        state_ref[...] = start_ref[...]
+        conv_ref[pl.ds(0, HEAD_ROWS), :] = jnp.zeros((HEAD_ROWS, size), f32)
+
+    @pl.when(pl.program_id(0) > 0)
+    def _():
+        conv_ref[pl.ds(0, HEAD_ROWS), :] = conv_ref[pl.ds(positions, HEAD_ROWS), :]
+
+    def exact(left, right, dims=((1,), (0,))):
+        return lax.dot_general(
+            left, right, (dims, ((), ())),
+            precision=lax.Precision.HIGHEST, preferred_element_type=f32,
+        )
+
+    def held(values):
+        return values.astype(bf16).astype(f32)
+
+    proj = None
+    for piece in range(pieces):
+        left = x_ref[:, piece].reshape(positions, depth)
+        term = jnp.dot(left, w_ref[piece], preferred_element_type=f32)
+        proj = term if proj is None else proj + term
+
+    def halves(index):
+        slab = proj[:, index * 2 * size : (index + 1) * 2 * size]
+        return held(slab[:, :size]), held(pltpu.roll(slab, size, 1)[:, :size])
+
+    query, keyed = halves(0)
+    valued, outer = halves(1)
+    inner, signal = halves(2)
+    rank = decay_map_ref.shape[0]
+    decay_low = jnp.tanh(proj[:, 6 * size : 6 * size + rank]).astype(bf16)
+    rate_low = proj[:, 6 * size + rank : 6 * size + 2 * rank].astype(bf16)
+    chan = chan_ref[...]
+    logits = (
+        chan[0:1]
+        + jnp.dot(decay_low, decay_map_ref[...], preferred_element_type=f32)
+        + pos_ref[...]
+    )
+    log_decay = -DECAY_FACTOR * jax.nn.sigmoid(logits) + extra_ref[...]
+    rate = jax.nn.sigmoid(
+        chan[1:2] + jnp.dot(rate_low, rate_map_ref[...], preferred_element_type=f32)
+    )
+    unit = keyed * lax.rsqrt(jnp.sum(keyed * keyed, axis=1, keepdims=True) + KEY_EPS)
+
+    mixed = held(inner * signal)
+    conv_ref[pl.ds(HEAD_ROWS, positions), :] = mixed
+    gated_ref[...] = outer * (
+        chan[4:5] * conv_ref[pl.ds(HEAD_ROWS - 2, positions), :]
+        + chan[5:6] * conv_ref[pl.ds(HEAD_ROWS - 1, positions), :]
+        + chan[6:7] * mixed
+    )
+
+    later = lax.broadcasted_iota(jnp.int32, (BLOCK, BLOCK), 0)
+    earlier = lax.broadcasted_iota(jnp.int32, (BLOCK, BLOCK), 1)
+    strict, inclusive = later > earlier, later >= earlier
+    eye = (later == earlier).astype(f32)
+    tri = inclusive.astype(f32)
+    every = range(count)
+
+    def cut(values):
+        return [values[g * BLOCK : (g + 1) * BLOCK] for g in every]
+
+    q, k, v, u, d = cut(query), cut(keyed), cut(valued), cut(unit), cut(log_decay)
+    ur = cut(unit * rate)
+    total = [exact(tri, d[g]) for g in every]
+    before = [total[g] - d[g] for g in every]
+    middle = [total[g][BLOCK // 2 - 1 : BLOCK // 2] for g in every]
+    closing = [total[g][BLOCK - 1 : BLOCK] for g in every]
+    fall = [jnp.exp(middle[g] - total[g]) for g in every]
+    left = [
+        jnp.concatenate(
+            [-u[g] * jnp.exp(before[g] - middle[g]), q[g] * jnp.exp(total[g] - middle[g])], axis=0
+        )
+        for g in every
+    ]
+    over_b = [exact(left[g], ur[g] * fall[g], ((1,), (1,))) for g in every]
+    over_k = [exact(left[g], k[g] * fall[g], ((1,), (1,))) for g in every]
+    removal = [jnp.where(strict, over_b[g][:BLOCK], 0.0) for g in every]
+    reads = [jnp.where(inclusive, over_b[g][BLOCK:], 0.0) for g in every]
+    on_values = [
+        exact(
+            jnp.concatenate(
+                [
+                    jnp.where(strict, over_k[g][:BLOCK], 0.0),
+                    jnp.where(inclusive, over_k[g][BLOCK:], 0.0),
+                ],
+                axis=0,
+            ),
+            v[g],
+        )
+        for g in every
+    ]
+    inverse = [eye + removal[g] for g in every]
+    power = [exact(removal[g], removal[g]) for g in every]
+    reach = 4
+    while reach < BLOCK:
+        both = [
+            exact(jnp.concatenate([inverse[g], power[g]], axis=0), power[g]) for g in every
+        ]
+        inverse = [inverse[g] + both[g][:BLOCK] for g in every]
+        power = [both[g][BLOCK:] for g in every]
+        reach = reach * 2
+    inverse = [inverse[g] + exact(inverse[g], power[g]) for g in every]
+    unit_solved = [exact(inverse[g], -u[g] * jnp.exp(before[g])) for g in every]
+    free_solved = [exact(inverse[g], on_values[g][:BLOCK]) for g in every]
+    probe = [q[g] * jnp.exp(total[g]) + exact(reads[g], unit_solved[g]) for g in every]
+    free_read = [exact(reads[g], free_solved[g]) + on_values[g][BLOCK:] for g in every]
+    rest = [jnp.exp(closing[g] - total[g]) for g in every]
+    b_end = [ur[g] * rest[g] for g in every]
+    k_end = [k[g] * rest[g] for g in every]
+    first = ((0,), (0,))
+    step = [
+        eye * jnp.exp(closing[g]) + exact(unit_solved[g], b_end[g], first) for g in every
+    ]
+    added = [
+        exact(free_solved[g], b_end[g], first) + exact(v[g], k_end[g], first) for g in every
+    ]
+    state = state_ref[...]
+    entering = []
+    for g in every:
+        entering.append(state)
+        state = exact(state, step[g]) + added[g]
+    state_ref[...] = state
+    recalled = jnp.concatenate(
+        [exact(probe[g], entering[g], ((1,), (1,))) + free_read[g] for g in every], axis=0
+    )
+    center = recalled - jnp.mean(recalled, axis=1, keepdims=True)
+    variance = jnp.mean(center * center, axis=1, keepdims=True)
+    own = jnp.sum(query * keyed * chan[2:3], axis=1, keepdims=True) * valued
+    lin_ref[...] = (center * lax.rsqrt(variance + GROUP_EPS) * chan[3:4] + own).astype(bf16)
+
+
+def run_head(gathered, weights, pos, extra, decay_map, rate_map, chan, start):
+    spans, pieces, rows, depth = gathered.shape
+    group = 2 if spans % 2 == 0 else 1
+    positions, size, rank = group * rows, start.shape[0], decay_map.shape[0]
+    length = spans * rows
+    width = weights.shape[2]
+
+    def fixed(shape):
+        return pl.BlockSpec(shape, lambda i: (0,) * len(shape))
+
+    def along(columns):
+        return pl.BlockSpec((positions, columns), lambda i: (i, 0))
+
+    return pl.pallas_call(
+        head_kernel,
+        grid=(spans // group,),
+        out_shape=(
+            jax.ShapeDtypeStruct((length, size), jnp.bfloat16),
+            jax.ShapeDtypeStruct((length, size), jnp.float32),
+        ),
+        in_specs=[
+            pl.BlockSpec((group, pieces, rows, depth), lambda i: (i, 0, 0, 0)),
+            fixed((pieces, depth, width)),
+            along(1),
+            along(1),
+            fixed((rank, size)),
+            fixed((rank, size)),
+            fixed(chan.shape),
+            fixed((size, size)),
+        ],
+        out_specs=(along(size), along(size)),
+        scratch_shapes=[
+            pltpu.VMEM((size, size), jnp.float32),
+            pltpu.VMEM((positions + HEAD_ROWS, size), jnp.float32),
+        ],
+        compiler_params=pltpu.CompilerParams(vmem_limit_bytes=56 * 1024 * 1024),
+        cost_estimate=pl.CostEstimate(
+            flops=2 * length * pieces * depth * width,
+            bytes_accessed=2 * length * pieces * depth,
+            transcendentals=0,
+        ),
+        name="head",
+    )(gathered, weights, pos, extra, decay_map, rate_map, chan, start)
+
+
+def per_head(
+    tokens,
+    input_norm_gain,
+    query_weight,
+    key_weight,
+    value_weight,
+    decay_first_map,
+    decay_second_map,
+    channel_decay_offset,
+    position_decay_offset,
+    extra_log_decay,
+    rate_first_map,
+    rate_second_map,
+    channel_rate_offset,
+    own_term_weight,
+    head_norm_gain,
+    starting_state,
+    outer_gate_weight,
+    inner_gate_weight,
+    signal_weight,
+    convolution_taps,
+    convolution_gain,
+):
+    devices, splits = lax.axis_size("sp"), lax.axis_size("tp")
+    mine, column = lax.axis_index("sp"), lax.axis_index("tp")
+    rows, depth = tokens.shape
+    features = depth * splits
+    size = starting_state.shape[2]
+    weights = jnp.stack(
+        [query_weight, key_weight, value_weight, outer_gate_weight, inner_gate_weight, signal_weight]
+    )
+    deep = query_weight.shape[0]
+    parcels = jnp.transpose(
+        weights.reshape(6, deep, devices, size), (2, 1, 0, 3)
+    ).reshape(devices, deep, 6 * size)
+    wide = tokens.astype(jnp.float32)
+    squares = lax.psum(jnp.sum(wide * wide, axis=1), "tp")
+    gain = lax.dynamic_slice(input_norm_gain, (column * depth,), (depth,))
+    normed = (wide * lax.rsqrt(squares[:, None] / features + NORM_EPS) * gain).astype(jnp.bfloat16)
+    moved = lax.all_to_all(parcels, "sp", 0, 0, tiled=True)
+    gathered = lax.all_gather(normed, ("sp", "tp"), axis=0, tiled=False)
+    small = lax.all_gather(
+        jnp.concatenate([position_decay_offset[:, None], extra_log_decay], axis=1),
+        "sp", axis=0, tiled=True,
+    )
+    pos = small[:, :1]
+    extra = lax.dynamic_slice(small, (0, 1 + mine), (small.shape[0], 1))
+    whole_weights = jnp.concatenate(
+        [moved.reshape(features, 6 * size), decay_first_map, rate_first_map], axis=1
+    ).reshape(splits, depth, -1)
+
+    def own(values):
+        return lax.dynamic_slice_in_dim(values, mine * size, size, axis=values.ndim - 1)
+
+    chan = jnp.stack(
+        [
+            own(channel_decay_offset),
+            own(channel_rate_offset),
+            own(own_term_weight),
+            own(head_norm_gain),
+            *own(convolution_taps).astype(jnp.float32),
+            own(convolution_gain),
+        ]
+    )
+    start = lax.dynamic_index_in_dim(starting_state, mine, 0, keepdims=False)
+    linear, gated = run_head(
+        gathered.reshape(devices, splits, rows, depth),
+        whole_weights, pos, extra, own(decay_second_map), own(rate_second_map), chan, start,
+    )
+    sums = lax.psum(jnp.sum(gated * gated, axis=1), ("sp", "tp"))
+    channels = size * devices * splits
+    conv = (gated * lax.rsqrt(sums[:, None] / channels + NORM_EPS) * chan[7]).astype(jnp.bfloat16)
+    back = lax.all_to_all(
+        jnp.concatenate([linear, conv], axis=1).reshape(devices, rows, 2 * size),
+        "sp", 0, 0, tiled=True,
+    )
+    back = jnp.transpose(back.reshape(devices, rows, 2, size), (2, 1, 0, 3))
+    back = back.reshape(2, rows, devices * size)
+    return (back[0], back[1])
+
+
+def plan(*arrays):
+    heads = arrays[15].shape[0]
+    if heads == lax.axis_size("sp") and arrays[0].shape[0] % BLOCK == 0:
+        return per_head(*arrays)
+    return shards(*arrays)
+
+
 def solution(mesh):
     placed = (
         P("sp", "tp"),
@@ -294,7 +578,7 @@
         P("tp"),
     )
     return jax.shard_map(
-        shards,
+        plan,
         mesh=mesh,
         in_specs=placed,
         out_specs=(P("sp", "tp"), P("sp", "tp")),

time: 519 us -> 326 us (0.63); the launches traced: 508 us -> 325 us
  waiting for transfers between devices: 301 us -> 22.8 us
  blocking collectives: 6.56 us -> 190 us
  matrix products: 81.4 us -> 0 us
  Pallas kernels: 0 us -> 54.7 us
  starting transfers between devices: 47.9 us -> 6 us
  other arithmetic: 35.6 us -> 14.4 us
    all_gather x7 -> x1, waiting for transfers between devices: 270 us -> 22.8 us  [per_head(): gathered = lax.all_gather(normed, ('sp', 'tp'), axis=0, tiled=False)]
    all_gather x0 -> x1, blocking collectives: none -> 124 us  [per_head(): lax.all_gather(jnp.concatenate([position_decay_offset[:, None], extra_log...]
    dot_general x49 -> x0, matrix products: 81.4 us -> none  [the longest x41 50.4 us: contract(): return jnp.einsum(spec, left, right, precision=lax.Precision.HIGHEST)]
    pallas_call x0 -> x1, Pallas kernels: none -> 54.7 us  [run_head(): pl.pallas_call(head_kernel, grid=(spans // group,), out_shape=(jax.ShapeD...]
    ppermute x8 -> x0, starting transfers between devices: 47.6 us -> none  [from_behind(): return lax.ppermute(block, axis, route)]
    psum x1 -> x2, blocking collectives: 6.56 us -> 46.3 us  [the longest x1 38 us: per_head(): sums = lax.psum(jnp.sum(gated * gated, axis=1), ('sp', 'tp'))]
    another operation x1 -> x0, other arithmetic: 26.4 us -> none  [mixer_blocks(): cumul = jnp.cumsum(decay_b, axis=1)]
    ppermute x8 -> x0, waiting for transfers between devices: 26.1 us -> none  [from_behind(): return lax.ppermute(block, axis, route)]
  transfers between devices with their start and end apart: 15 -> 2, of which waited for: 14 -> 1; matrix products, arithmetic and copies ran while one was open for 27% -> 8% of each run, Pallas kernels for 0% -> 0%
where the time goes in v1:
time: 326 us; the launch traced here: 325 us
  blocking collectives  190 us (58%)
  Pallas kernels  54.7 us (17%)
  local copies, waits for them, and re-layouts  23 us (7%)
  waiting for transfers between devices  22.8 us (7%)
  other arithmetic  14.4 us (4%)
  between operations  14.2 us (4%)
  starting transfers between devices  6 us (2%)
    all_gather x1, blocking collectives, per_head(): lax.all_gather(jnp.concatenate([position_decay_offset[:, None], extra_log...  124 us
    pallas_call x1, Pallas kernels, run_head(): pl.pallas_call(head_kernel, grid=(spans // group,), out_shape=(jax.ShapeD...  54.7 us
    psum x1, blocking collectives, per_head(): sums = lax.psum(jnp.sum(gated * gated, axis=1), ('sp', 'tp'))  38 us
    all_gather x1, waiting for transfers between devices, per_head(): gathered = lax.all_gather(normed, ('sp', 'tp'), axis=0, tiled=False)  22.8 us
    all_to_all x1, blocking collectives, per_head(): lax.all_to_all(jnp.concatenate([linear, conv], axis=1).reshape(devices, r...  19.4 us
    psum x1, blocking collectives, per_head(): squares = lax.psum(jnp.sum(wide * wide, axis=1), 'tp')  8.37 us
    unnamed x25, local copies, waits for them, and re-layouts  7.39 us
  transfers between devices with their start and end apart: 2, of which 1 were waited for; matrix products, arithmetic and copies ran while one was open for 8% of the time, Pallas kernels for 0%

profile of v1, /device:TPU:0, one launch (start us, length us, event | category | flops | bytes accessed | tf_op | source)
XLA Modules:
  0.0 324.8 jit_solution(466664060192071135)
XLA Ops:
  7.2 0.0 copy-start
  7.2 0.0 copy-start.1
  7.2 0.0 copy-start.2
  7.2 0.0 all-gather.3.cloned.1.call-start
  7.3 1.3 fusion
  8.6 8.4 %psum.14 = f32[256]{0:T(256)S(1)} all-reduce(f32[256]{0:T(256)S(1)} %fusion), channel_id=1, replica_groups=mesh['sp'=8,'tp'=4] {'tp'}, use_global_device_ids=true, to_apply=%region_1.0 | all-reduce | flops 256 | bytes 2048 | tf_op jit(solution)/shard_map/psum | solution.py:504
  16.9 0.7 dynamic_slice.34
  17.6 2.0 fusion.2
  19.7 0.0 all-gather.3.cloned.1.call-update
  19.7 1.3 copy.39
  21.0 0.0 copy-done.1
  21.0 0.2 copy.40
  21.2 0.0 copy-done.2
  21.2 0.2 copy.41
  21.4 1.3 copy.42
  22.7 1.3 copy.43
  23.9 1.3 copy.44
  25.5 0.1 constant_dynamic-update-slice_fusion
  25.5 2.0 copy.45
  27.5 6.0 %all-to-all-start = ((bf16[8,512,384]{1,2,0:T(8,128)(2,1)}), bf16[8,512,384]{1,2,0:T(8,128)(2,1)S(1)}, u32[]{:S(2)}, u32[]{:S(2)}) async-start(bf16[8,512,384]{1,2,0:T(8,128)(2,1)} %bitcast.31), calls=%async_computation | async-start | bytes 6291456 | tf_op jit(solution)/shard_map/all_to_all | solution.py:507
  33.5 0.0 copy-done.3
  33.5 0.0 copy-done.4
  33.5 0.1 copy.47
  33.6 1.3 dynamic_slice.43
  34.9 1.3 dynamic-slice_bitcast_fusion.5
  36.2 0.8 dynamic-slice_bitcast_fusion.3
  37.0 1.3 dynamic-slice_bitcast_fusion.1
  38.3 0.7 fusion.3
  39.0 1.3 stack.51.chan_ref
  40.3 123.9 %all_gather.11 = f32[2048,9]{1,0:T(8,128)S(1)} all-gather(f32[256,9]{1,0:T(8,128)S(1)} %copy.47), channel_id=1, replica_groups=mesh['sp'=8,'tp'=4] {'sp'}, dimensions={0}, use_global_device_ids=true | all-gather | bytes 82944 | tf_op jit(solution)/shard_map/all_gather | solution.py:509
  164.2 0.0 copy-done
  164.2 0.6 dynamic-slice_bitcast_fusion.start_ref
  164.8 1.5 constant_dynamic-slice_fusion.1
  166.3 1.7 constant_dynamic-slice_fusion.3
  168.0 0.0 all-to-all-done
  168.0 2.8 copy.46
  170.9 5.8 %pad_maximum_fusion.w_ref = bf16[4,1024,640]{2,1,0:T(8,128)(2,1)} fusion(bf16[4,1024,128]{2,1,0:T(8,128)(2,1)} %bitcast.42, bf16[4,1024,128]{2,1,0:T(8,128)(2,1)} %bitcast.43, bf16[4,1024,384]{2,1,0:T(8,128)(2,1)} %bitcast.32), kind=kLoop, calls=%fused_computation | loop fusion | flops 15728640 | bytes 10485760 | tf_op jit(solution)/shard_map/concatenate | solution.py:515
  176.7 22.8 %all-gather.3.cloned.1.call-done = bf16[8192,1024]{1,0:T(8,128)(2,1)} async-done(((bf16[256,1024]{1,0:T(8,128)(2,1)}), bf16[8192,1024]{1,0:T(8,128)(2,1)}) %all-gather.3.cloned.1.call-update) | async-done | bytes 16777232 | tf_op jit(solution)/shard_map/all_gather | solution.py:508
  199.5 54.7 %head.1 = (bf16[2048,64]{1,0:T(8,128)(2,1)}, f32[2048,64]{1,0:T(8,128)}) custom-call(bf16[8,4,256,1024]{3,2,1,0:T(8,128)(2,1)} %bitcast.47, bf16[4,1024,640]{2,1,0:T(8,128)(2,1)} %pad_maximum_fusion.w_ref, f32[2048,1]{1,0:T(8,128)} %get-tuple-element.11.pos_ref, f32[2048,1]{1,0:T(8,128)} %get-tuple-element.10.extra_ref, ...), custom_call_target="tpu_custom_call" | custom-call | flops 10737418240 | bytes 16777216 | tf_op jit(solution)/shard_map/head/pallas_call | solution.py:436
  254.2 1.6 multiply_reduce_fusion
  255.7 38.0 %psum.15 = f32[2048]{0:T(1024)S(1)} all-reduce(f32[2048]{0:T(1024)S(1)} %multiply_reduce_fusion), channel_id=1, replica_groups=mesh['sp'=8,'tp'=4] {'sp','tp'}, use_global_device_ids=true, to_apply=%region_3.4 | all-reduce | flops 2048 | bytes 16384 | tf_op jit(solution)/shard_map/psum | solution.py:537
  293.7 0.0 copy-done.5
  293.7 1.6 multiply_convert_fusion
  295.3 1.3 pad_maximum_fusion.1
  296.6 0.2 copy.48
  296.8 19.4 %all_to_all.10 = bf16[8,256,128]{1,2,0:T(8,128)(2,1)S(1)} all-to-all(bf16[8,256,128]{1,2,0:T(8,128)(2,1)S(1)} %copy.48), channel_id=1, replica_groups=mesh['sp'=8,'tp'=4] {'sp'}, dimensions={0} | all-to-all | bytes 1048576 | tf_op jit(solution)/shard_map/all_to_all | solution.py:540
  316.3 0.8 copy.49
  317.1 0.8 copy.50
  (12 shorter events, 0.3 us)
Async XLA Ops:
  7.2 157.1 %copy-start = (f32[8,64,64]{2,1,0:T(8,128)S(1)}, f32[8,64,64]{2,1,0:T(8,128)}, u32[]{:S(2)}) copy-start(f32[8,64,64]{2,1,0:T(8,128)} %param.36) | copy-start | bytes 393220
  7.2 13.8 %copy-start.1 = (bf16[512,512]{1,0:T(8,128)(2,1)S(1)}, bf16[512,512]{1,0:T(8,128)(2,1)}, u32[]{:S(2)}) copy-start(bf16[512,512]{1,0:T(8,128)(2,1)} %param.24) | copy-start | bytes 1572868
  7.2 14.0 %copy-start.2 = (bf16[512,512]{1,0:T(8,128)(2,1)S(1)}, bf16[512,512]{1,0:T(8,128)(2,1)}, u32[]{:S(2)}) copy-start(bf16[512,512]{1,0:T(8,128)(2,1)} %param.25) | copy-start | bytes 1572868
  7.2 192.3 %all-gather.3.cloned.1.call-start = ((), (), s32[]{:S(2)}) async-start(), calls=%async_computation.2 | async-start | bytes 17301504 | tf_op jit(solution)/shard_map/all_gather | solution.py:508
  27.5 6.0 %copy-start.3 = (f32[256,8]{0,1:T(8,128)S(1)}, f32[256,8]{0,1:T(8,128)}, u32[]{:S(2)}) copy-start(f32[256,8]{0,1:T(8,128)} %param.30) | copy-start | bytes 24580
  27.5 6.0 %copy-start.4 = (f32[256]{0:T(256)S(1)}, f32[256]{0:T(256)}, u32[]{:S(2)}) copy-start(f32[256]{0:T(256)} %param.29) | copy-start | bytes 3076
  27.5 140.5 %all-to-all-start = ((bf16[8,512,384]{1,2,0:T(8,128)(2,1)}), bf16[8,512,384]{1,2,0:T(8,128)(2,1)S(1)}, u32[]{:S(2)}, u32[]{:S(2)}) async-start(bf16[8,512,384]{1,2,0:T(8,128)(2,1)} %bitcast.31), calls=%async_computation | async-start | bytes 6291456 | tf_op jit(solution)/shard_map/all_to_all | solution.py:507
  199.5 94.2 %copy-start.5 = (f32[64]{0:T(128)S(1)}, f32[64]{0:T(128)}, u32[]{:S(2)}) copy-start(f32[64]{0:T(128)} %dynamic_slice.43) | copy-start | bytes 772
Sparse Core Ops, SparseCore 0:
  19.8 179.5 all-gather.2

commit v2 on v1

--- a/solution.py
+++ b/solution.py
@@ -295,10 +295,15 @@
     def _():
         conv_ref[pl.ds(0, HEAD_ROWS), :] = conv_ref[pl.ds(positions, HEAD_ROWS), :]
 
+    def once(left, right, dims):
+        return lax.dot_general(left, right, (dims, ((), ())), preferred_element_type=f32)
+
     def exact(left, right, dims=((1,), (0,))):
-        return lax.dot_general(
-            left, right, (dims, ((), ())),
-            precision=lax.Precision.HIGHEST, preferred_element_type=f32,
+        left_high, right_high = left.astype(bf16), right.astype(bf16)
+        left_low = (left - left_high.astype(f32)).astype(bf16)
+        right_low = (right - right_high.astype(f32)).astype(bf16)
+        return once(left_high, right_high, dims) + (
+            once(left_high, right_low, dims) + once(left_low, right_high, dims)
         )
 
     def held(values):
@@ -334,11 +339,12 @@
 
     mixed = held(inner * signal)
     conv_ref[pl.ds(HEAD_ROWS, positions), :] = mixed
-    gated_ref[...] = outer * (
+    gated = outer * (
         chan[4:5] * conv_ref[pl.ds(HEAD_ROWS - 2, positions), :]
         + chan[5:6] * conv_ref[pl.ds(HEAD_ROWS - 1, positions), :]
         + chan[6:7] * mixed
     )
+    gated_ref[...] = gated.astype(bf16)
 
     later = lax.broadcasted_iota(jnp.int32, (BLOCK, BLOCK), 0)
     earlier = lax.broadcasted_iota(jnp.int32, (BLOCK, BLOCK), 1)
@@ -352,7 +358,10 @@
 
     q, k, v, u, d = cut(query), cut(keyed), cut(valued), cut(unit), cut(log_decay)
     ur = cut(unit * rate)
-    total = [exact(tri, d[g]) for g in every]
+    total = [
+        jnp.dot(tri, d[g], precision=lax.Precision.HIGHEST, preferred_element_type=f32)
+        for g in every
+    ]
     before = [total[g] - d[g] for g in every]
     middle = [total[g][BLOCK // 2 - 1 : BLOCK // 2] for g in every]
     closing = [total[g][BLOCK - 1 : BLOCK] for g in every]
@@ -422,7 +431,7 @@
 
 def run_head(gathered, weights, pos, extra, decay_map, rate_map, chan, start):
     spans, pieces, rows, depth = gathered.shape
-    group = 2 if spans % 2 == 0 else 1
+    group = 1
     positions, size, rank = group * rows, start.shape[0], decay_map.shape[0]
     length = spans * rows
     width = weights.shape[2]
@@ -438,7 +447,7 @@
         grid=(spans // group,),
         out_shape=(
             jax.ShapeDtypeStruct((length, size), jnp.bfloat16),
-            jax.ShapeDtypeStruct((length, size), jnp.float32),
+            jax.ShapeDtypeStruct((length, size), jnp.bfloat16),
         ),
         in_specs=[
             pl.BlockSpec((group, pieces, rows, depth), lambda i: (i, 0, 0, 0)),
@@ -526,7 +535,7 @@
             own(own_term_weight),
             own(head_norm_gain),
             *own(convolution_taps).astype(jnp.float32),
-            own(convolution_gain),
+            jnp.zeros((size,), jnp.float32),
         ]
     )
     start = lax.dynamic_index_in_dim(starting_state, mine, 0, keepdims=False)
@@ -534,16 +543,17 @@
         gathered.reshape(devices, splits, rows, depth),
         whole_weights, pos, extra, own(decay_second_map), own(rate_second_map), chan, start,
     )
-    sums = lax.psum(jnp.sum(gated * gated, axis=1), ("sp", "tp"))
-    channels = size * devices * splits
-    conv = (gated * lax.rsqrt(sums[:, None] / channels + NORM_EPS) * chan[7]).astype(jnp.bfloat16)
     back = lax.all_to_all(
-        jnp.concatenate([linear, conv], axis=1).reshape(devices, rows, 2 * size),
+        jnp.concatenate([linear, gated], axis=1).reshape(devices, rows, 2 * size),
         "sp", 0, 0, tiled=True,
     )
     back = jnp.transpose(back.reshape(devices, rows, 2, size), (2, 1, 0, 3))
     back = back.reshape(2, rows, devices * size)
-    return (back[0], back[1])
+    gated = back[1].astype(jnp.float32)
+    sums = lax.psum(jnp.sum(gated * gated, axis=1), "tp")
+    channels = size * devices * splits
+    conv = gated * lax.rsqrt(sums[:, None] / channels + NORM_EPS) * convolution_gain
+    return (back[0], conv.astype(jnp.bfloat16))
 
 
 def plan(*arrays):

time: 326 us -> 278 us (0.85)
  blocking collectives: 190 us -> 159 us
  Pallas kernels: 54.7 us -> 42.6 us
    psum x1, blocking collectives: 38 us -> 5.63 us  [per_head(): sums = lax.psum(jnp.sum(gated * gated, axis=1), 'tp')]
    pallas_call x1, Pallas kernels: 54.7 us -> 42.6 us  [run_head(): pl.pallas_call(head_kernel, grid=(spans // group,), out_shape=(jax.ShapeD...]
  transfers between devices with their start and end apart: 2 -> 2, of which waited for: 1 -> 1; matrix products, arithmetic and copies ran while one was open for 8% -> 9% of each run, Pallas kernels for 0% -> 0%
where the time goes in v2:
time: 278 us; the launch traced here: 277 us
  blocking collectives  159 us (57%)
  Pallas kernels  42.6 us (15%)
  waiting for transfers between devices  22.7 us (8%)
  local copies, waits for them, and re-layouts  21 us (8%)
  between operations  14.2 us (5%)
  other arithmetic  11.8 us (4%)
  starting transfers between devices  6 us (2%)
    all_gather x1, blocking collectives, per_head(): lax.all_gather(jnp.concatenate([position_decay_offset[:, None], extra_log...  126 us
    pallas_call x1, Pallas kernels, run_head(): pl.pallas_call(head_kernel, grid=(spans // group,), out_shape=(jax.ShapeD...  42.6 us
    all_gather x1, waiting for transfers between devices, per_head(): gathered = lax.all_gather(normed, ('sp', 'tp'), axis=0, tiled=False)  22.7 us
    all_to_all x1, blocking collectives, per_head(): lax.all_to_all(jnp.concatenate([linear, gated], axis=1).reshape(devices,...  18.6 us
    psum x1, blocking collectives, per_head(): squares = lax.psum(jnp.sum(wide * wide, axis=1), 'tp')  8.37 us
    unnamed x25, local copies, waits for them, and re-layouts  7.39 us
    all_to_all x1, starting transfers between devices, per_head(): moved = lax.all_to_all(parcels, 'sp', 0, 0, tiled=True)  5.97 us
    concatenate x1, other arithmetic, per_head(): jnp.concatenate([moved.reshape(features, 6 * size), decay_first_map, rate...  5.83 us
  transfers between devices with their start and end apart: 2, of which 1 were waited for; matrix products, arithmetic and copies ran while one was open for 9% of the time, Pallas kernels for 0%

profile of v2, /device:TPU:0, one launch (start us, length us, event | category | flops | bytes accessed | tf_op | source)
XLA Modules:
  0.0 276.9 jit_solution(13197643237033522886)
XLA Ops:
  7.2 0.0 copy-start
  7.2 0.0 copy-start.1
  7.2 0.0 copy-start.2
  7.2 0.0 all-gather.3.cloned.1.call-start
  7.3 1.3 fusion
  8.6 8.4 %psum.14 = f32[256]{0:T(256)S(1)} all-reduce(f32[256]{0:T(256)S(1)} %fusion), channel_id=1, replica_groups=mesh['sp'=8,'tp'=4] {'tp'}, use_global_device_ids=true, to_apply=%region_1.0 | all-reduce | flops 256 | bytes 2048 | tf_op jit(solution)/shard_map/psum | solution.py:513
  16.9 0.7 dynamic_slice.31
  17.6 2.0 fusion.2
  19.7 0.0 all-gather.3.cloned.1.call-update
  19.7 1.3 copy.39
  21.0 0.0 copy-done.1
  21.0 0.2 copy.40
  21.2 0.0 copy-done.2
  21.2 0.2 copy.41
  21.4 1.3 copy.42
  22.7 1.3 copy.43
  23.9 1.3 copy.44
  25.5 0.1 constant_dynamic-update-slice_fusion
  25.5 2.0 copy.45
  27.5 6.0 %all-to-all-start = ((bf16[8,512,384]{1,2,0:T(8,128)(2,1)}), bf16[8,512,384]{1,2,0:T(8,128)(2,1)S(1)}, u32[]{:S(2)}, u32[]{:S(2)}) async-start(bf16[8,512,384]{1,2,0:T(8,128)(2,1)} %bitcast.34), calls=%async_computation | async-start | bytes 6291456 | tf_op jit(solution)/shard_map/all_to_all | solution.py:516
  33.5 0.0 copy-done.3
  33.5 0.0 copy-done.5
  33.5 0.1 copy.47
  33.6 0.8 dynamic-slice_bitcast_fusion.3
  34.4 1.3 dynamic-slice_bitcast_fusion.1
  35.7 0.7 fusion.5
  36.5 0.5 stack_broadcast_in_dim.3
  37.0 1.3 stack.47.chan_ref
  38.2 126.0 %all_gather.11 = f32[2048,9]{1,0:T(8,128)S(1)} all-gather(f32[256,9]{1,0:T(8,128)S(1)} %copy.47), channel_id=1, replica_groups=mesh['sp'=8,'tp'=4] {'sp'}, dimensions={0}, use_global_device_ids=true | all-gather | bytes 82944 | tf_op jit(solution)/shard_map/all_gather | solution.py:518
  164.3 0.0 copy-done
  164.3 0.6 dynamic-slice_bitcast_fusion.start_ref
  164.9 1.5 constant_dynamic-slice_fusion.1
  166.4 1.7 constant_dynamic-slice_fusion.3
  168.0 0.0 all-to-all-done
  168.0 2.8 %copy.46 = bf16[8,512,384]{2,1,0:T(8,128)(2,1)} copy(bf16[8,512,384]{1,2,0:T(8,128)(2,1)S(1)} %all-to-all-done) | data formatting | bytes 6291456 | tf_op jit(solution)/shard_map/all_to_all | solution.py:516
  170.9 5.8 %pad_maximum_fusion.w_ref = bf16[4,1024,640]{2,1,0:T(8,128)(2,1)} fusion(bf16[4,1024,128]{2,1,0:T(8,128)(2,1)} %bitcast.46, bf16[4,1024,128]{2,1,0:T(8,128)(2,1)} %bitcast.47, bf16[4,1024,384]{2,1,0:T(8,128)(2,1)} %bitcast.35), kind=kLoop, calls=%fused_computation | loop fusion | flops 15728640 | bytes 10485760 | tf_op jit(solution)/shard_map/concatenate | solution.py:524
  176.7 22.7 %all-gather.3.cloned.1.call-done = bf16[8192,1024]{1,0:T(8,128)(2,1)} async-done(((bf16[256,1024]{1,0:T(8,128)(2,1)}), bf16[8192,1024]{1,0:T(8,128)(2,1)}) %all-gather.3.cloned.1.call-update) | async-done | bytes 16777232 | tf_op jit(solution)/shard_map/all_gather | solution.py:517
  199.4 42.6 %head.1 = (bf16[2048,64]{1,0:T(8,128)(2,1)}, bf16[2048,64]{1,0:T(8,128)(2,1)}) custom-call(bf16[8,4,256,1024]{3,2,1,0:T(8,128)(2,1)} %bitcast.50, bf16[4,1024,640]{2,1,0:T(8,128)(2,1)} %pad_maximum_fusion.w_ref, f32[2048,1]{1,0:T(8,128)} %get-tuple-element.11.pos_ref, f32[2048,1]{1,0:T(8,128)} %get-tuple-element.10.extra_ref, ...), custom_call_target="tpu_custom_call" | custom-call | flops 10737418240 | bytes 16777216 | tf_op jit(solution)/shard_map/head/pallas_call | solution.py:445
  242.1 1.5 pad_maximum_fusion.1
  243.6 0.2 copy.48
  243.8 18.6 %all_to_all.10 = bf16[8,256,128]{1,2,0:T(8,128)(2,1)S(1)} all-to-all(bf16[8,256,128]{1,2,0:T(8,128)(2,1)S(1)} %copy.48), channel_id=1, replica_groups=mesh['sp'=8,'tp'=4] {'sp'}, dimensions={0} | all-to-all | bytes 1048576 | tf_op jit(solution)/shard_map/all_to_all | solution.py:546
  262.4 0.1 slice_convert_fusion
  262.5 0.1 multiply_reduce_fusion
  262.6 0.8 copy.49
  263.4 5.6 %psum.15 = f32[256]{0:T(256)S(1)} all-reduce(f32[256]{0:T(256)S(1)} %multiply_reduce_fusion), channel_id=1, replica_groups=mesh['sp'=8,'tp'=4] {'tp'}, use_global_device_ids=true, to_apply=%region_3.4 | all-reduce | flops 256 | bytes 2048 | tf_op jit(solution)/shard_map/psum | solution.py:553
  269.0 0.0 copy-done.4
  269.0 0.1 fusion.4
  269.2 0.8 copy.50
  (11 shorter events, 0.3 us)
Async XLA Ops:
  7.2 157.1 %copy-start = (f32[8,64,64]{2,1,0:T(8,128)S(1)}, f32[8,64,64]{2,1,0:T(8,128)}, u32[]{:S(2)}) copy-start(f32[8,64,64]{2,1,0:T(8,128)} %param.36) | copy-start | bytes 393220
  7.2 13.8 %copy-start.1 = (bf16[512,512]{1,0:T(8,128)(2,1)S(1)}, bf16[512,512]{1,0:T(8,128)(2,1)}, u32[]{:S(2)}) copy-start(bf16[512,512]{1,0:T(8,128)(2,1)} %param.24) | copy-start | bytes 1572868
  7.2 14.0 %copy-start.2 = (bf16[512,512]{1,0:T(8,128)(2,1)S(1)}, bf16[512,512]{1,0:T(8,128)(2,1)}, u32[]{:S(2)}) copy-start(bf16[512,512]{1,0:T(8,128)(2,1)} %param.25) | copy-start | bytes 1572868
  7.2 192.2 %all-gather.3.cloned.1.call-start = ((), (), s32[]{:S(2)}) async-start(), calls=%async_computation.2 | async-start | bytes 17301504 | tf_op jit(solution)/shard_map/all_gather | solution.py:517
  27.5 6.0 %copy-start.3 = (f32[256,8]{0,1:T(8,128)S(1)}, f32[256,8]{0,1:T(8,128)}, u32[]{:S(2)}) copy-start(f32[256,8]{0,1:T(8,128)} %param.30) | copy-start | bytes 24580
  27.5 6.0 %copy-start.5 = (f32[256]{0:T(256)S(1)}, f32[256]{0:T(256)}, u32[]{:S(2)}) copy-start(f32[256]{0:T(256)} %param.29) | copy-start | bytes 3076
  27.5 140.5 %all-to-all-start = ((bf16[8,512,384]{1,2,0:T(8,128)(2,1)}), bf16[8,512,384]{1,2,0:T(8,128)(2,1)S(1)}, u32[]{:S(2)}, u32[]{:S(2)}) async-start(bf16[8,512,384]{1,2,0:T(8,128)(2,1)} %bitcast.34), calls=%async_computation | async-start | bytes 6291456 | tf_op jit(solution)/shard_map/all_to_all | solution.py:516
  242.1 26.9 %copy-start.4 = (f32[512]{0:T(512)S(1)}, f32[512]{0:T(512)}, u32[]{:S(2)}) copy-start(f32[512]{0:T(512)} %param.41) | copy-start | bytes 6148
Sparse Core Ops, SparseCore 0:
  19.8 179.5 all-gather.2
